TPU v7x, 32 devices: a whole 2x2x4 slice. The times are simulated.
32 devices in a mesh: ep: 8 (over z, core), tp: 4 (over y, x).
Axes of the slice: x: 2, y: 2, z: 4, core: 2. Of those that a mesh axis runs over, the one named last changes fastest.
Arguments:
- q_latent: bfloat16 [4096, 512], P('ep'), may hold values from -6 to 6
- kv_latent: bfloat16 [4096, 256], P('ep'), may hold values from -6 to 6
- rope_key: bfloat16 [4096, 32], P('ep'), may hold values from -400 to 400
- q_gain: bfloat16 [512], replicated, may hold values from 0.099609375 to 1.8984375
- kv_gain: bfloat16 [256], replicated, may hold values from 0.099609375 to 1.8984375
- w_q_nope: bfloat16 [512, 1024], P(None, 'tp'), may hold values from -0.25 to 0.25
- w_q_rope: bfloat16 [512, 512], P(None, 'tp'), may hold values from -0.25 to 0.25
- w_k_nope: bfloat16 [256, 1024], P(None, 'tp'), may hold values from -0.375 to 0.375
- w_value: bfloat16 [256, 1024], P(None, 'tp'), may hold values from -0.375 to 0.375
- w_out: bfloat16 [1024, 2048], P('tp'), may hold values from -5.375 to 5.375
- tokens_b: bfloat16 [1024, 2048], P('ep'), may hold values from -6 to 6
- norm_gain_b: bfloat16 [2048], replicated, may hold values from 0.099609375 to 1.8984375
- routes: int32 [1024, 2], P('ep'), may hold values from 0 to 7, all different within a row; in each aligned block of 128 rows (0 to 127, 128 to 255, ...) at most 48 rows name the same one
- route_logits: float32 [1024, 2], P('ep'), may hold values from -6 to 6
- w_gate: bfloat16 [8, 2048, 4096], P('ep', None, 'tp'), may hold values from -0.125 to 0.125
- w_up: bfloat16 [8, 2048, 4096], P('ep', None, 'tp'), may hold values from -0.125 to 0.125
- w_down: bfloat16 [8, 4096, 2048], P('ep', 'tp'), may hold values from -0.125 to 0.125
Outputs:
- mixer_out: bfloat16 [4096, 2048], P(('ep', 'tp'))
- expert_mix: bfloat16 [1024, 2048], P('ep', 'tp')
Inputs may be any that keep to these rules, and one draw needn't show every extreme that they name: `routes`: each row names two different experts. In each aligned block of 128 rows (the rows of one index of ep) no expert is named by more than 48 rows, and in every draw some expert is named by exactly 48 rows of some block.
All inputs are finite; a program needn't handle non-finite values.
Results may differ from a plain program's by a relative error of at most 0.022.
The roundings to bfloat16 on the way count: a program that leaves them out, or rounds other values in their place, can miss the bound.
Values may be sent and summed in bfloat16 or wider, within the bound.
A program may use at most 128 MiB of HBM per device.

v0:
```python
import jax
import jax.numpy as jnp
from jax import lax
from jax.sharding import PartitionSpec as P

NOPE = 64
ROPE = 32
VDIM = 64
EPSILON = 1e-06
FLOOR = -1e30


def rms_rows(values, gain):
    wide = values.astype(jnp.float32)
    scaled = wide * lax.rsqrt(jnp.mean(wide * wide, axis=-1, keepdims=True) + EPSILON)
    return (scaled * gain.astype(jnp.float32)).astype(jnp.bfloat16)


def rotate(values, places):
    half = values.shape[-1] // 2
    freqs = 10000.0 ** (-jnp.arange(half, dtype=jnp.float32) / half)
    angles = places.astype(jnp.float32)[:, None] * freqs[None, :]
    cosine = jnp.cos(angles)[:, None, :]
    sine = jnp.sin(angles)[:, None, :]
    first = values[..., :half]
    second = values[..., half:]
    return jnp.concatenate(
        [first * cosine - second * sine, first * sine + second * cosine], axis=-1
    )


def key_side(kv_piece, rope_piece, kv_gain, w_k_nope, w_value):
    count = kv_piece.shape[0]
    places = jnp.arange(count, dtype=jnp.int32)
    normed = rms_rows(kv_piece, kv_gain)
    k_nope = jnp.dot(normed, w_k_nope, preferred_element_type=jnp.float32).astype(jnp.bfloat16)
    values = jnp.dot(normed, w_value, preferred_element_type=jnp.float32).astype(jnp.bfloat16)
    k_rope = rotate(rope_piece.astype(jnp.float32)[:, None, :], places)[:, 0].astype(jnp.bfloat16)
    return (k_nope, values, k_rope)


def attend_block(carry, q_nope, q_rope, k_nope, values, k_rope):
    top, total_w, acc = carry
    heads = q_nope.shape[1]
    count = k_nope.shape[0]
    key_heads = k_nope.reshape(count, heads, NOPE)
    value_heads = values.reshape(count, heads, VDIM)
    scores = jnp.einsum("qhd,khd->hqk", q_nope, key_heads, preferred_element_type=jnp.float32)
    scores = scores + jnp.einsum("qhr,kr->hqk", q_rope, k_rope, preferred_element_type=jnp.float32)
    scores = scores * (NOPE + ROPE) ** (-0.5)
    new_top = jnp.maximum(top, jnp.max(scores, axis=-1))
    shrink = jnp.exp(top - new_top)
    weights = jnp.exp(scores - new_top[..., None])
    total_w = total_w * shrink + jnp.sum(weights, axis=-1)
    acc = acc * shrink[..., None] + jnp.einsum(
        "hqk,khd->hqd",
        weights.astype(jnp.bfloat16),
        value_heads,
        preferred_element_type=jnp.float32,
    )
    return (new_top, total_w, acc)


def attend(carry, q_nope, q_rope, k_nope, values, k_rope):
    count = k_nope.shape[0]
    span = 512

    def advance(state, pieces):
        return (attend_block(state, q_nope, q_rope, pieces[0], pieces[1], pieces[2]), None)

    blocks = (
        k_nope.reshape(count // span, span, k_nope.shape[1]),
        values.reshape(count // span, span, values.shape[1]),
        k_rope.reshape(count // span, span, k_rope.shape[1]),
    )
    carry, _ = lax.scan(advance, carry, blocks)
    return carry


def shards(
    q_latent,
    kv_latent,
    rope_key,
    q_gain,
    kv_gain,
    w_q_nope,
    w_q_rope,
    w_k_nope,
    w_value,
    w_out,
    tokens_b,
    norm_gain_b,
    routes,
    route_logits,
    w_gate,
    w_up,
    w_down,
):
    own_rows = q_latent.shape[0]
    heads = w_q_nope.shape[1] // NOPE
    offset = lax.axis_index("ep") * own_rows
    places = offset + jnp.arange(own_rows, dtype=jnp.int32)
    q_normed = rms_rows(q_latent, q_gain)
    q_nope = jnp.dot(q_normed, w_q_nope, preferred_element_type=jnp.float32).astype(jnp.bfloat16)
    q_nope = q_nope.reshape(own_rows, heads, NOPE)
    q_turn = jnp.dot(q_normed, w_q_rope, preferred_element_type=jnp.float32).reshape(
        own_rows, heads, ROPE
    )
    q_rope = rotate(q_turn, places).astype(jnp.bfloat16)
    start_carry = (
        jnp.full((heads, own_rows), FLOOR, jnp.float32),
        jnp.zeros((heads, own_rows), jnp.float32),
        jnp.zeros((heads, own_rows, VDIM), jnp.float32),
    )
    piece_keys, piece_values, piece_rotary = key_side(
        lax.all_gather(kv_latent, "ep", axis=0, tiled=True),
        lax.all_gather(rope_key, "ep", axis=0, tiled=True),
        kv_gain,
        w_k_nope,
        w_value,
    )
    top, total_w, acc = attend(start_carry, q_nope, q_rope, piece_keys, piece_values, piece_rotary)
    attended = (acc / total_w[..., None]).astype(jnp.bfloat16)
    attended = attended.transpose(1, 0, 2).reshape(own_rows, heads * VDIM)
    rows = attended
    mixer_out = lax.psum_scatter(
        jnp.dot(rows, w_out, preferred_element_type=jnp.float32).astype(jnp.bfloat16),
        "tp",
        scatter_dimension=0,
        tiled=True,
    )
    n_ep = lax.axis_size("ep")
    n_tp = lax.axis_size("tp")
    rows_b = tokens_b.shape[0]
    width = tokens_b.shape[1]
    room = 3 * rows_b // n_ep
    normed_b = rms_rows(tokens_b, norm_gain_b)
    weights_b = jax.nn.softmax(route_logits, axis=-1)
    flat = routes.reshape(-1)
    assigned = flat.shape[0]
    onehot = (flat[:, None] == jnp.arange(n_ep, dtype=jnp.int32)[None, :]).astype(jnp.int32)
    slot = jnp.sum((jnp.cumsum(onehot, axis=0) - 1) * onehot, axis=1)
    where = flat * room + slot
    table = (
        jnp.full((n_ep * room,), assigned, jnp.int32)
        .at[where]
        .set(jnp.arange(assigned, dtype=jnp.int32))
    )
    padded = jnp.concatenate([normed_b, jnp.zeros((1, width), jnp.bfloat16)], axis=0)
    share = width // n_tp
    narrow_rows = lax.dynamic_slice_in_dim(padded, lax.axis_index("tp") * share, share, 1)
    outgoing = narrow_rows[table // 2].reshape(n_ep, room, share)
    arrived = lax.all_to_all(outgoing, "ep", split_axis=0, concat_axis=0, tiled=True)
    sources, count, piece_width = arrived.shape
    rows = arrived.reshape(sources * count, piece_width)
    piece = lax.all_gather(rows, "tp", axis=1, tiled=True)
    gate_rows = w_gate[0]
    up_rows = w_up[0]
    gate = jnp.dot(piece, gate_rows, preferred_element_type=jnp.float32)
    up = jnp.dot(piece, up_rows, preferred_element_type=jnp.float32)
    hidden = (jax.nn.silu(gate) * up).astype(jnp.bfloat16)
    term = jnp.dot(hidden, w_down[0], preferred_element_type=jnp.float32)
    summed = lax.psum_scatter(
        term.astype(jnp.bfloat16), "tp", scatter_dimension=1, tiled=True
    ).astype(jnp.float32)
    finished = summed.astype(jnp.bfloat16).reshape(sources, count, summed.shape[1])
    back = lax.all_to_all(finished, "ep", split_axis=0, concat_axis=0, tiled=True)
    back = back.reshape(n_ep * room, back.shape[2])
    picked = back[where.reshape(rows_b, 2)].astype(jnp.float32)
    expert_mix = jnp.sum(picked * weights_b[:, :, None], axis=1).astype(jnp.bfloat16)
    return (mixer_out, expert_mix)


def solution(mesh):
    placed = (
        P("ep", None),
        P("ep", None),
        P("ep", None),
        P(),
        P(),
        P(None, "tp"),
        P(None, "tp"),
        P(None, "tp"),
        P(None, "tp"),
        P("tp", None),
        P("ep", None),
        P(),
        P("ep", None),
        P("ep", None),
        P("ep", None, "tp"),
        P("ep", None, "tp"),
        P("ep", "tp", None),
    )
    return jax.shard_map(
        shards,
        mesh=mesh,
        in_specs=placed,
        out_specs=(P(("ep", "tp"), None), P("ep", "tp")),
        check_vma=False,
    )
```

profile of v0, /device:TPU:0, one launch (start us, length us, event | category | flops | bytes accessed | tf_op | source)
XLA Modules:
  0.0 233.3 jit_solution(3116432101885813936)
XLA Ops:
  16.4 18.9 %all_to_all.10 = bf16[8,48,512]{2,1,0:T(8,128)(2,1)} all-to-all(bf16[8,48,512]{2,1,0:T(8,128)(2,1)S(1)} %bitcast.88), channel_id=1, replica_groups=mesh['ep'=8,'tp'=4] {'ep'}, dimensions={0} | all-to-all | bytes 786432 | tf_op jit(solution)/shard_map/all_to_all | solution.py:153
  36.2 14.2 %all_gather.10 = bf16[4096,32]{0,1:T(8,128)(2,1)S(1)} all-gather(bf16[512,32]{0,1:T(8,128)(2,1)S(1)} %copy-done.3), channel_id=1, replica_groups=mesh['ep'=8,'tp'=4] {'ep'}, dimensions={0}, use_global_device_ids=true | all-gather | bytes 294912 | tf_op jit(solution)/shard_map/all_gather | solution.py:117
  53.3 11.9 %all-gather.5.cloned.1.call-done = bf16[384,2048]{1,0:T(8,128)(2,1)} async-done(((bf16[384,512]{1,0:T(8,128)(2,1)}), bf16[384,2048]{1,0:T(8,128)(2,1)}) %all-gather.5.cloned.1.call-update) | async-done | bytes 1572880 | tf_op jit(solution)/shard_map/all_gather | solution.py:156
  65.2 5.6 %fusion.20 = f32[384,1024]{1,0:T(8,128)} fusion(bf16[384,2048]{1,0:T(8,128)(2,1)} %all-gather.5.cloned.1.call-done, bf16[1,2048,1024]{2,1,0:T(8,128)(2,1)} %param.33), kind=kOutput, calls=%fused_computation.32 | convolution fusion | flops 1610612736 | bytes 7340032 | tf_op jit(solution)/shard_map/dot_general | solution.py:159
  70.8 9.5 %fusion.22 = bf16[384,2048]{1,0:T(8,128)(2,1)} fusion(bf16[1,1024,2048]{2,1,0:T(8,128)(2,1)} %param.35, f32[384,1024]{1,0:T(8,128)} %fusion.20, bf16[384,2048]{1,0:T(8,128)(2,1)} %all-gather.5.cloned.1.call-done, bf16[1,2048,1024]{2,1,0:T(8,128)(2,1)} %param.34), kind=kOutput, calls=%fused_computation.35 | convolution fusion | flops 3224371200 | bytes 13107200 | tf_op jit(solution)/shard_map/dot_general | solution.py:162
  80.6 15.4 %all-gather.3.cloned.1.call-done = bf16[4096,256]{1,0:T(8,128)(2,1)} async-done(((bf16[512,256]{1,0:T(8,128)(2,1)}), bf16[4096,256]{1,0:T(8,128)(2,1)}) %all-gather.3.cloned.1.call-update) | async-done | bytes 2097168 | tf_op jit(solution)/shard_map/all_gather | solution.py:116
  98.4 3.7 %convolution_convert_fusion.1 = bf16[4096,256]{1,0:T(8,128)(2,1)} fusion(bf16[256,256]{1,0:T(8,128)(2,1)S(1)} %copy-done.8, bf16[4096,256]{1,0:T(8,128)(2,1)} %all-gather.3.cloned.1.call-done, f32[256]{0:T(256)S(1)} %convert_element_type.92, f32[4096]{0:T(1024)S(1)} %add_rsqrt_fusion), kind=kOutput, calls=%fused_computation.24 | convolution fusion | flops 542113792 | bytes 4342784 | tf_op jit(solution)/shard_map/dot_general | solution.py:36
  104.0 85.6 %while.15 = (s32[]{:T(128)}, f32[4,512]{1,0:T(4,128)S(1)}, f32[4,512]{1,0:T(4,128)S(1)}, f32[4,512,64]{1,2,0:T(8,128)S(1)}, bf16[8,512,256]{2,1,0:T(8,128)(2,1)}...) while((s32[]{:T(128)}, f32[4,512]{1,0:T(4,128)S(1)}, ...), condition=%wide.region_5.6_spmd.clone, body=%wide.region_2.5_spmd.clone.sunk | while | flops 343287808 | bytes 25198728 | solution.py:76
  108.8 2.9 %fusion.89 = f32[4,512]{1,0:T(4,128)S(1)} fusion(f32[4,512,512]{1,2,0:T(8,128)} %get-tuple-element.195, f32[4,512]{1,0:T(4,128)S(1)} %select_maximum_fusion.2), kind=kLoop, calls=%fused_computation.7.clone.1 | loop fusion | flops 2095104 | bytes 4210688 | tf_op jit(solution)/shard_map/while/body/eval_jaxpr/reduce_sum | solution.py:54
  111.9 3.1 %fusion.91 = f32[4,512,64]{1,2,0:T(8,128)S(1)} fusion(bf16[512,4,64]{0,2,1:T(8,128)(2,1)S(1)} %bitcast.82, f32[4,512,512]{1,2,0:T(8,128)} %get-tuple-element.195, f32[4,512]{1,0:T(4,128)S(1)} %select_maximum_fusion.2, f32[4,512,64]{1,2,0:T(8,128)S(1)} %get-tuple-element.213, f32[4,512]{1,0:T(4,128)S(1)} %get-tuple-element.198, pred[]{:T(512)S(6)} %compare.6), kind=kOutput, calls=%fused_computation.10.clone.1 | convolution fusion | flops 136708096 | bytes 5521409 | tf_op jit(solution)/shard_map/while/body/eval_jaxpr/hqk,khd->hqd/dot_general | solution.py:55
  119.7 2.8 %fusion.89 = f32[4,512]{1,0:T(4,128)S(1)} fusion(f32[4,512,512]{1,2,0:T(8,128)} %get-tuple-element.195, f32[4,512]{1,0:T(4,128)S(1)} %select_maximum_fusion.2), kind=kLoop, calls=%fused_computation.7.clone.1 | loop fusion | flops 2095104 | bytes 4210688 | tf_op jit(solution)/shard_map/while/body/eval_jaxpr/reduce_sum | solution.py:54
  122.6 3.0 %fusion.91 = f32[4,512,64]{1,2,0:T(8,128)S(1)} fusion(bf16[512,4,64]{0,2,1:T(8,128)(2,1)S(1)} %bitcast.82, f32[4,512,512]{1,2,0:T(8,128)} %get-tuple-element.195, f32[4,512]{1,0:T(4,128)S(1)} %select_maximum_fusion.2, f32[4,512,64]{1,2,0:T(8,128)S(1)} %get-tuple-element.213, f32[4,512]{1,0:T(4,128)S(1)} %get-tuple-element.198, pred[]{:T(512)S(6)} %compare.6), kind=kOutput, calls=%fused_computation.10.clone.1 | convolution fusion | flops 136708096 | bytes 5521409 | tf_op jit(solution)/shard_map/while/body/eval_jaxpr/hqk,khd->hqd/dot_general | solution.py:55
  130.3 2.8 %fusion.89 = f32[4,512]{1,0:T(4,128)S(1)} fusion(f32[4,512,512]{1,2,0:T(8,128)} %get-tuple-element.195, f32[4,512]{1,0:T(4,128)S(1)} %select_maximum_fusion.2), kind=kLoop, calls=%fused_computation.7.clone.1 | loop fusion | flops 2095104 | bytes 4210688 | tf_op jit(solution)/shard_map/while/body/eval_jaxpr/reduce_sum | solution.py:54
  133.3 3.0 %fusion.91 = f32[4,512,64]{1,2,0:T(8,128)S(1)} fusion(bf16[512,4,64]{0,2,1:T(8,128)(2,1)S(1)} %bitcast.82, f32[4,512,512]{1,2,0:T(8,128)} %get-tuple-element.195, f32[4,512]{1,0:T(4,128)S(1)} %select_maximum_fusion.2, f32[4,512,64]{1,2,0:T(8,128)S(1)} %get-tuple-element.213, f32[4,512]{1,0:T(4,128)S(1)} %get-tuple-element.198, pred[]{:T(512)S(6)} %compare.6), kind=kOutput, calls=%fused_computation.10.clone.1 | convolution fusion | flops 136708096 | bytes 5521409 | tf_op jit(solution)/shard_map/while/body/eval_jaxpr/hqk,khd->hqd/dot_general | solution.py:55
  143.9 3.0 %fusion.91 = f32[4,512,64]{1,2,0:T(8,128)S(1)} fusion(bf16[512,4,64]{0,2,1:T(8,128)(2,1)S(1)} %bitcast.82, f32[4,512,512]{1,2,0:T(8,128)} %get-tuple-element.195, f32[4,512]{1,0:T(4,128)S(1)} %select_maximum_fusion.2, f32[4,512,64]{1,2,0:T(8,128)S(1)} %get-tuple-element.213, f32[4,512]{1,0:T(4,128)S(1)} %get-tuple-element.198, pred[]{:T(512)S(6)} %compare.6), kind=kOutput, calls=%fused_computation.10.clone.1 | convolution fusion | flops 136708096 | bytes 5521409 | tf_op jit(solution)/shard_map/while/body/eval_jaxpr/hqk,khd->hqd/dot_general | solution.py:55
  151.7 2.8 %fusion.89 = f32[4,512]{1,0:T(4,128)S(1)} fusion(f32[4,512,512]{1,2,0:T(8,128)} %get-tuple-element.195, f32[4,512]{1,0:T(4,128)S(1)} %select_maximum_fusion.2), kind=kLoop, calls=%fused_computation.7.clone.1 | loop fusion | flops 2095104 | bytes 4210688 | tf_op jit(solution)/shard_map/while/body/eval_jaxpr/reduce_sum | solution.py:54
  154.6 3.0 %fusion.91 = f32[4,512,64]{1,2,0:T(8,128)S(1)} fusion(bf16[512,4,64]{0,2,1:T(8,128)(2,1)S(1)} %bitcast.82, f32[4,512,512]{1,2,0:T(8,128)} %get-tuple-element.195, f32[4,512]{1,0:T(4,128)S(1)} %select_maximum_fusion.2, f32[4,512,64]{1,2,0:T(8,128)S(1)} %get-tuple-element.213, f32[4,512]{1,0:T(4,128)S(1)} %get-tuple-element.198, pred[]{:T(512)S(6)} %compare.6), kind=kOutput, calls=%fused_computation.10.clone.1 | convolution fusion | flops 136708096 | bytes 5521409 | tf_op jit(solution)/shard_map/while/body/eval_jaxpr/hqk,khd->hqd/dot_general | solution.py:55
  165.3 3.0 %fusion.91 = f32[4,512,64]{1,2,0:T(8,128)S(1)} fusion(bf16[512,4,64]{0,2,1:T(8,128)(2,1)S(1)} %bitcast.82, f32[4,512,512]{1,2,0:T(8,128)} %get-tuple-element.195, f32[4,512]{1,0:T(4,128)S(1)} %select_maximum_fusion.2, f32[4,512,64]{1,2,0:T(8,128)S(1)} %get-tuple-element.213, f32[4,512]{1,0:T(4,128)S(1)} %get-tuple-element.198, pred[]{:T(512)S(6)} %compare.6), kind=kOutput, calls=%fused_computation.10.clone.1 | convolution fusion | flops 136708096 | bytes 5521409 | tf_op jit(solution)/shard_map/while/body/eval_jaxpr/hqk,khd->hqd/dot_general | solution.py:55
  175.9 3.0 %fusion.91 = f32[4,512,64]{1,2,0:T(8,128)S(1)} fusion(bf16[512,4,64]{0,2,1:T(8,128)(2,1)S(1)} %bitcast.82, f32[4,512,512]{1,2,0:T(8,128)} %get-tuple-element.195, f32[4,512]{1,0:T(4,128)S(1)} %select_maximum_fusion.2, f32[4,512,64]{1,2,0:T(8,128)S(1)} %get-tuple-element.213, f32[4,512]{1,0:T(4,128)S(1)} %get-tuple-element.198, pred[]{:T(512)S(6)} %compare.6), kind=kOutput, calls=%fused_computation.10.clone.1 | convolution fusion | flops 136708096 | bytes 5521409 | tf_op jit(solution)/shard_map/while/body/eval_jaxpr/hqk,khd->hqd/dot_general | solution.py:55
  183.6 2.8 %fusion.89 = f32[4,512]{1,0:T(4,128)S(1)} fusion(f32[4,512,512]{1,2,0:T(8,128)} %get-tuple-element.195, f32[4,512]{1,0:T(4,128)S(1)} %select_maximum_fusion.2), kind=kLoop, calls=%fused_computation.7.clone.1 | loop fusion | flops 2095104 | bytes 4210688 | tf_op jit(solution)/shard_map/while/body/eval_jaxpr/reduce_sum | solution.py:54
  186.6 3.0 %fusion.91 = f32[4,512,64]{1,2,0:T(8,128)S(1)} fusion(bf16[512,4,64]{0,2,1:T(8,128)(2,1)S(1)} %bitcast.82, f32[4,512,512]{1,2,0:T(8,128)} %get-tuple-element.195, f32[4,512]{1,0:T(4,128)S(1)} %select_maximum_fusion.2, f32[4,512,64]{1,2,0:T(8,128)S(1)} %get-tuple-element.213, f32[4,512]{1,0:T(4,128)S(1)} %get-tuple-element.198, pred[]{:T(512)S(6)} %compare.6), kind=kOutput, calls=%fused_computation.10.clone.1 | convolution fusion | flops 136708096 | bytes 5521409 | tf_op jit(solution)/shard_map/while/body/eval_jaxpr/hqk,khd->hqd/dot_general | solution.py:55
  191.9 3.5 %all-to-all-start.1 = ((bf16[8,48,512]{2,1,0:T(8,128)(2,1)}), bf16[8,48,512]{2,1,0:T(8,128)(2,1)S(1)}, u32[]{:S(2)}, u32[]{:S(2)}) async-start(bf16[8,48,512]{2,1,0:T(8,128)(2,1)} %bitcast.93), calls=%async_computation.3 | async-start | bytes 786432 | tf_op jit(solution)/shard_map/all_to_all | solution.py:167
  195.7 12.1 %all-to-all-done.1 = bf16[8,48,512]{2,1,0:T(8,128)(2,1)S(1)} async-done(((bf16[8,48,512]{2,1,0:T(8,128)(2,1)}), bf16[8,48,512]{2,1,0:T(8,128)(2,1)S(1)}, u32[]{:S(2)}, u32[]{:S(2)}) %all-to-all-start.1) | async-done | bytes 393248 | tf_op jit(solution)/shard_map/all_to_all | solution.py:167
  210.7 16.1 %reduce-scatter.3.cloned.1.call-done = bf16[128,2048]{1,0:T(8,128)(2,1)} async-done(((bf16[512,2048]{1,0:T(8,128)(2,1)}), bf16[128,2048]{1,0:T(8,128)(2,1)}) %reduce-scatter.3.cloned.1.call-update) | async-done | bytes 524304 | tf_op jit(solution)/shard_map/reduce_scatter | solution.py:126
  (155 shorter events, 69.4 us)
Async XLA Ops:
  7.2 182.6 %copy-start = (bf16[256,2048]{1,0:T(8,128)(2,1)S(1)}, bf16[256,2048]{1,0:T(8,128)(2,1)}, u32[]{:S(2)}) copy-start(bf16[256,2048]{1,0:T(8,128)(2,1)} %param.28) | copy-start | bytes 3145732
  7.2 29.0 %copy-start.3 = (bf16[512,32]{0,1:T(8,128)(2,1)S(1)}, bf16[512,32]{0,1:T(8,128)(2,1)}, u32[]{:S(2)}) copy-start(bf16[512,32]{0,1:T(8,128)(2,1)} %param.21) | copy-start | bytes 98308
  7.2 58.0 %all-gather.5.cloned.1.call-start = ((), (), s32[]{:S(2)}) async-start(), calls=%async_computation.6 | async-start | bytes 1966080 | tf_op jit(solution)/shard_map/all_gather | solution.py:156
  13.0 38.6 %copy-start.10 = (bf16[256]{0:T(256)(128)(2,1)S(1)}, bf16[256]{0:T(256)(128)(2,1)}, u32[]{:S(2)}) copy-start(bf16[256]{0:T(256)(128)(2,1)} %param.23) | copy-start | bytes 1540
  13.0 38.6 %copy-start.5 = (bf16[512]{0:T(512)(128)(2,1)S(1)}, bf16[512]{0:T(512)(128)(2,1)}, u32[]{:S(2)}) copy-start(bf16[512]{0:T(512)(128)(2,1)} %param.22) | copy-start | bytes 3076
  14.3 37.6 %copy-start.2 = (bf16[512,512]{1,0:T(8,128)(2,1)S(1)}, bf16[512,512]{1,0:T(8,128)(2,1)}, u32[]{:S(2)}) copy-start(bf16[512,512]{1,0:T(8,128)(2,1)} %param.19) | copy-start | bytes 1572868
  14.3 38.0 %copy-start.7 = (bf16[512,128]{1,0:T(8,128)(2,1)S(1)}, bf16[512,128]{1,0:T(8,128)(2,1)}, u32[]{:S(2)}) copy-start(bf16[512,128]{1,0:T(8,128)(2,1)} %param.25) | copy-start | bytes 393220
  16.4 36.4 %copy-start.6 = (bf16[512,256]{1,0:T(8,128)(2,1)S(1)}, bf16[512,256]{1,0:T(8,128)(2,1)}, u32[]{:S(2)}) copy-start(bf16[512,256]{1,0:T(8,128)(2,1)} %param.24) | copy-start | bytes 786436
  35.4 60.6 %all-gather.3.cloned.1.call-start = ((), (), s32[]{:S(2)}) async-start(), calls=%async_computation.4 | async-start | bytes 2359296 | tf_op jit(solution)/shard_map/all_gather | solution.py:116
  36.1 155.8 %reduce-scatter.5.cloned.1.call-start = ((), (), s32[]{:S(2)}) async-start(), calls=%async_computation.7 | async-start | bytes 1966080 | tf_op jit(solution)/shard_map/reduce_scatter | solution.py:163
  70.8 27.5 %copy-start.8 = (bf16[256,256]{1,0:T(8,128)(2,1)S(1)}, bf16[256,256]{1,0:T(8,128)(2,1)}, u32[]{:S(2)}) copy-start(bf16[256,256]{1,0:T(8,128)(2,1)} %param.26) | copy-start | bytes 393220
  80.3 21.8 %copy-start.9 = (bf16[256,256]{1,0:T(8,128)(2,1)S(1)}, bf16[256,256]{1,0:T(8,128)(2,1)}, u32[]{:S(2)}) copy-start(bf16[256,256]{1,0:T(8,128)(2,1)} %param.27) | copy-start | bytes 393220
  80.3 146.4 %reduce-scatter.3.cloned.1.call-start = ((), (), s32[]{:S(2)}) async-start(), calls=%async_computation.5 | async-start | bytes 2621440 | tf_op jit(solution)/shard_map/reduce_scatter | solution.py:126
  96.0 6.1 %copy-start.1 = (bf16[4096,256]{1,0:T(8,128)(2,1)S(1)}, bf16[4096,256]{1,0:T(8,128)(2,1)}, u32[]{:S(2)}) copy-start(bf16[4096,256]{1,0:T(8,128)(2,1)} %all-gather.3.cloned.1.call-done) | copy-start | bytes 6291460
  189.6 5.9 %copy-start.4 = (f32[128,2]{0,1:T(2,128)S(1)}, f32[128,2]{0,1:T(2,128)}, u32[]{:S(2)}) copy-start(f32[128,2]{0,1:T(2,128)} %param.32) | copy-start | bytes 3076
  191.9 15.9 %all-to-all-start.1 = ((bf16[8,48,512]{2,1,0:T(8,128)(2,1)}), bf16[8,48,512]{2,1,0:T(8,128)(2,1)S(1)}, u32[]{:S(2)}, u32[]{:S(2)}) async-start(bf16[8,48,512]{2,1,0:T(8,128)(2,1)} %bitcast.93), calls=%async_computation.3 | async-start | bytes 786432 | tf_op jit(solution)/shard_map/all_to_all | solution.py:167
Sparse Core Ops, SparseCore 0:
  35.5 29.6 all-gather.4
  66.8 29.1 all-gather.2
  99.0 30.5 reduce-scatter.4
  192.0 34.7 reduce-scatter.2
where the time goes:
time: 234 us; the launch traced here: 233 us
  matrix products  75.6 us (32%)
  waiting for transfers between devices  56.3 us (24%)
  blocking collectives  33.1 us (14%)
  other arithmetic  31.9 us (14%)
  local copies, waits for them, and re-layouts  18 us (8%)
  between operations  14.2 us (6%)
  starting transfers between devices  3.8 us (2%)
    dot_general x8, matrix products, attend_block(): jnp.einsum('hqk,khd->hqd', weights.astype(jnp.bfloat16), value_heads, pre...  24.4 us
    reduce_sum x8, other arithmetic, attend_block(): total_w = total_w * shrink + jnp.sum(weights, axis=-1)  22.2 us
    dot_general x8, matrix products, attend_block(): jnp.einsum('qhr,kr->hqk', q_rope, k_rope, preferred_element_type=jnp.floa...  21.3 us
    all_to_all x1, blocking collectives, shards(): lax.all_to_all(outgoing, 'ep', split_axis=0, concat_axis=0, tiled=True)  18.9 us
    reduce_scatter x1, waiting for transfers between devices, shards(): lax.psum_scatter(jnp.dot(rows, w_out, preferred_element_type=jnp.float32)...  16.1 us
    all_gather x1, waiting for transfers between devices, shards(): lax.all_gather(kv_latent, 'ep', axis=0, tiled=True)  15.4 us
    all_gather x1, blocking collectives, shards(): lax.all_gather(rope_key, 'ep', axis=0, tiled=True)  14.2 us
    all_to_all x1, waiting for transfers between devices, shards(): lax.all_to_all(finished, 'ep', split_axis=0, concat_axis=0, tiled=True)  12.1 us
  transfers between devices with their start and end apart: 5, of which 4 were waited for; matrix products, arithmetic and copies ran while one was open for 50% of the time, Pallas kernels for 0%

commit v1 on v0

--- a/solution.py
+++ b/solution.py
@@ -8,6 +8,16 @@
 VDIM = 64
 EPSILON = 1e-06
 FLOOR = -1e30
+
+
+def pass_along(x, name, dim):
+    count = lax.axis_size(name)
+    held, blocks = (x, [x])
+    for _ in range(count - 1):
+        held = lax.ppermute(held, name, [(i, (i + 1) % count) for i in range(count)])
+        blocks.insert(0, held)
+    line = jnp.concatenate(blocks, axis=dim)
+    return jnp.roll(line, (lax.axis_index(name) + 1) * x.shape[dim], axis=dim)
 
 
 def rms_rows(values, gain):
@@ -153,7 +163,7 @@
     arrived = lax.all_to_all(outgoing, "ep", split_axis=0, concat_axis=0, tiled=True)
     sources, count, piece_width = arrived.shape
     rows = arrived.reshape(sources * count, piece_width)
-    piece = lax.all_gather(rows, "tp", axis=1, tiled=True)
+    piece = pass_along(rows, "tp", 1)
     gate_rows = w_gate[0]
     up_rows = w_up[0]
     gate = jnp.dot(piece, gate_rows, preferred_element_type=jnp.float32)

time: 234 us -> 250 us (1.068)
  starting transfers between devices: 3.8 us -> 13.1 us
  blocking collectives: 33.1 us -> 29.6 us
  matrix products: 75.6 us -> 78.9 us
  local copies, waits for them, and re-layouts: 18 us -> 21.1 us
  other arithmetic: 31.9 us -> 34.7 us
    ppermute x0 -> x3, waiting for transfers between devices: none -> 26 us  [pass_along(): lax.ppermute(held, name, [(i, (i + 1) % count) for i in range(count)])]
    all_to_all x1 -> x0, blocking collectives: 18.9 us -> none  [shards(): lax.all_to_all(outgoing, 'ep', split_axis=0, concat_axis=0, tiled=True)]
    all_gather x1, waiting for transfers between devices: 15.4 us -> 0.02 us  [shards(): lax.all_gather(kv_latent, 'ep', axis=0, tiled=True)]
    all_gather x1, blocking collectives: 14.2 us -> 29.6 us  [shards(): lax.all_gather(rope_key, 'ep', axis=0, tiled=True)]
    all_gather x1 -> x0, waiting for transfers between devices: 11.9 us -> none  [shards(): piece = lax.all_gather(rows, 'tp', axis=1, tiled=True)]
    all_to_all x0 -> x1, starting transfers between devices: none -> 6.35 us  [shards(): lax.all_to_all(outgoing, 'ep', split_axis=0, concat_axis=0, tiled=True)]
    dot_general x8, matrix products: 21.3 us -> 27.4 us  [attend_block(): jnp.einsum('qhr,kr->hqk', q_rope, k_rope, preferred_element_type=jnp.floa...]
    dot_general x1, matrix products: 5.63 us -> 1.82 us  [shards(): gate = jnp.dot(piece, gate_rows, preferred_element_type=jnp.float32)]
  transfers between devices with their start and end apart: 5 -> 8, of which waited for: 4 -> 5; matrix products, arithmetic and copies ran while one was open for 50% -> 54% of each run, Pallas kernels for 0% -> 0%
where the time goes in v1:
time: 250 us; the launch traced here: 248 us
  matrix products  78.9 us (32%)
  waiting for transfers between devices  54.1 us (22%)
  other arithmetic  34.7 us (14%)
  blocking collectives  29.6 us (12%)
  local copies, waits for them, and re-layouts  21.1 us (8%)
  between operations  16 us (6%)
  starting transfers between devices  13.1 us (5%)
    all_gather x1, blocking collectives, shards(): lax.all_gather(rope_key, 'ep', axis=0, tiled=True)  29.6 us
    dot_general x8, matrix products, attend_block(): jnp.einsum('qhr,kr->hqk', q_rope, k_rope, preferred_element_type=jnp.floa...  27.4 us
    ppermute x3, waiting for transfers between devices, pass_along(): lax.ppermute(held, name, [(i, (i + 1) % count) for i in range(count)])  26 us
    dot_general x8, matrix products, attend_block(): jnp.einsum('hqk,khd->hqd', weights.astype(jnp.bfloat16), value_heads, pre...  24.4 us
    reduce_sum x8, other arithmetic, attend_block(): total_w = total_w * shrink + jnp.sum(weights, axis=-1)  22.2 us
    reduce_scatter x1, waiting for transfers between devices, shards(): lax.psum_scatter(jnp.dot(rows, w_out, preferred_element_type=jnp.float32)...  15.2 us
    all_to_all x1, waiting for transfers between devices, shards(): lax.all_to_all(finished, 'ep', split_axis=0, concat_axis=0, tiled=True)  12.2 us
    dynamic_slice x24, local copies, waits for them, and re-layouts, attend(): carry, _ = lax.scan(advance, carry, blocks)  10.8 us
  transfers between devices with their start and end apart: 8, of which 5 were waited for; matrix products, arithmetic and copies ran while one was open for 54% of the time, Pallas kernels for 0%

profile of v1, /device:TPU:0, one launch (start us, length us, event | category | flops | bytes accessed | tf_op | source)
XLA Modules:
  0.0 248.0 jit_solution(10703727478610666950)
XLA Ops:
  19.0 6.4 %all-to-all-start = ((bf16[8,48,512]{2,1,0:T(8,128)(2,1)}), bf16[8,48,512]{2,1,0:T(8,128)(2,1)S(1)}, u32[]{:S(2)}, u32[]{:S(2)}) async-start(bf16[8,48,512]{2,1,0:T(8,128)(2,1)} %bitcast.12), calls=%async_computation.1 | async-start | bytes 786432 | tf_op jit(solution)/shard_map/all_to_all | solution.py:163
  25.6 29.6 %all_gather.7 = bf16[4096,32]{0,1:T(8,128)(2,1)S(1)} all-gather(bf16[512,32]{0,1:T(8,128)(2,1)S(1)} %copy-done.5), channel_id=1, replica_groups=mesh['ep'=8,'tp'=4] {'ep'}, dimensions={0}, use_global_device_ids=true | all-gather | bytes 294912 | tf_op jit(solution)/shard_map/all_gather | solution.py:127
  59.3 9.4 %collective-permute-done = bf16[384,512]{1,0:T(8,128)(2,1)S(1)} collective-permute-done((bf16[384,512]{1,0:T(8,128)(2,1)S(1)}, bf16[384,512]{1,0:T(8,128)(2,1)S(1)}, u32[]{:S(2)}, u32[]{:S(2)}) %collective-permute-start) | collective-permute-done | bytes 393248 | tf_op jit(solution)/shard_map/ppermute | solution.py:17
  69.4 10.8 %collective-permute-done.1 = bf16[384,512]{1,0:T(8,128)(2,1)S(1)} collective-permute-done((bf16[384,512]{1,0:T(8,128)(2,1)S(1)}, bf16[384,512]{1,0:T(8,128)(2,1)S(1)}, u32[]{:S(2)}, u32[]{:S(2)}) %collective-permute-start.1) | collective-permute-done | bytes 393248 | tf_op jit(solution)/shard_map/ppermute | solution.py:17
  85.0 5.8 %collective-permute-done.2 = bf16[384,512]{1,0:T(8,128)(2,1)S(1)} collective-permute-done((bf16[384,512]{1,0:T(8,128)(2,1)S(1)}, bf16[384,512]{1,0:T(8,128)(2,1)S(1)}, u32[]{:S(2)}, u32[]{:S(2)}) %collective-permute-start.2) | collective-permute-done | bytes 393248 | tf_op jit(solution)/shard_map/ppermute | solution.py:17
  94.7 8.8 %fusion.22 = bf16[384,2048]{1,0:T(8,128)(2,1)} fusion(bf16[1,1024,2048]{2,1,0:T(8,128)(2,1)} %param.35, f32[384,1024]{1,0:T(8,128)S(1)} %fusion.20, bf16[1,2048,1024]{2,1,0:T(8,128)(2,1)} %param.34, bf16[384,4096]{1,0:T(8,128)(2,1)} %copy-done.4, s32[]{:T(128)S(6)} %select_n.42), kind=kOutput, calls=%fused_computation.35 | convolution fusion | flops 3224371200 | bytes 13107204 | tf_op jit(solution)/shard_map/dot_general | solution.py:172
  106.2 3.7 %convolution_convert_fusion.1 = bf16[4096,256]{1,0:T(8,128)(2,1)} fusion(bf16[256,256]{1,0:T(8,128)(2,1)S(1)} %copy-done.12, bf16[4096,256]{1,0:T(8,128)(2,1)} %all-gather.2.cloned.1.call-done, f32[256]{0:T(256)S(1)} %copy-done.14, f32[4096]{0:T(1024)S(1)} %add_rsqrt_fusion), kind=kOutput, calls=%fused_computation.24 | convolution fusion | flops 542113792 | bytes 4342784 | tf_op jit(solution)/shard_map/dot_general | solution.py:46
  111.8 91.5 %while.15 = (s32[]{:T(128)}, f32[4,512]{1,0:T(4,128)S(1)}, f32[4,512]{1,0:T(4,128)S(1)}, f32[4,512,64]{1,2,0:T(8,128)S(1)}, bf16[8,512,256]{2,1,0:T(8,128)(2,1)}...) while((s32[]{:T(128)}, f32[4,512]{1,0:T(4,128)S(1)}, ...), condition=%wide.region_5.6_spmd.clone, body=%wide.region_2.5_spmd.clone.sunk | while | flops 343287808 | bytes 25198728 | solution.py:86
  113.8 3.4 %fusion.95 = (f32[4,512]{1,0:T(4,128)S(1)}, f32[4,512,512]{1,2,0:T(8,128)}) fusion(bf16[512,4,32]{0,2,1:T(8,128)(2,1)S(1)} %get-tuple-element.228, bf16[8,512,32]{1,2,0:T(8,128)(2,1)} %get-tuple-element.227, s32[]{:T(128)S(6)} %copy.43, f32[4,512,512]{2,1,0:T(8,128)S(1)} %fusion.94), kind=kOutput, calls=%fused_computation.113.clone.1 | convolution fusion | flops 70252544 | bytes 8560644 | tf_op jit(solution)/shard_map/while/body/eval_jaxpr/qhr,kr->hqk/dot_general | solution.py:59
  120.3 3.1 %fusion.98 = f32[4,512,64]{1,2,0:T(8,128)S(1)} fusion(bf16[512,4,64]{0,2,1:T(8,128)(2,1)S(1)} %bitcast.80, f32[4,512,512]{1,2,0:T(8,128)} %get-tuple-element.195, f32[4,512]{1,0:T(4,128)S(1)} %select_maximum_fusion.2, f32[4,512,64]{1,2,0:T(8,128)S(1)} %get-tuple-element.213, f32[4,512]{1,0:T(4,128)S(1)} %get-tuple-element.198, pred[]{:T(512)S(6)} %compare.7), kind=kOutput, calls=%fused_computation.10.clone.1 | convolution fusion | flops 136708096 | bytes 5521409 | tf_op jit(solution)/shard_map/while/body/eval_jaxpr/hqk,khd->hqd/dot_general | solution.py:65
  125.4 3.4 %fusion.95 = (f32[4,512]{1,0:T(4,128)S(1)}, f32[4,512,512]{1,2,0:T(8,128)}) fusion(bf16[512,4,32]{0,2,1:T(8,128)(2,1)S(1)} %get-tuple-element.228, bf16[8,512,32]{1,2,0:T(8,128)(2,1)} %get-tuple-element.227, s32[]{:T(128)S(6)} %copy.43, f32[4,512,512]{2,1,0:T(8,128)S(1)} %fusion.94), kind=kOutput, calls=%fused_computation.113.clone.1 | convolution fusion | flops 70252544 | bytes 8560644 | tf_op jit(solution)/shard_map/while/body/eval_jaxpr/qhr,kr->hqk/dot_general | solution.py:59
  131.7 3.1 %fusion.98 = f32[4,512,64]{1,2,0:T(8,128)S(1)} fusion(bf16[512,4,64]{0,2,1:T(8,128)(2,1)S(1)} %bitcast.80, f32[4,512,512]{1,2,0:T(8,128)} %get-tuple-element.195, f32[4,512]{1,0:T(4,128)S(1)} %select_maximum_fusion.2, f32[4,512,64]{1,2,0:T(8,128)S(1)} %get-tuple-element.213, f32[4,512]{1,0:T(4,128)S(1)} %get-tuple-element.198, pred[]{:T(512)S(6)} %compare.7), kind=kOutput, calls=%fused_computation.10.clone.1 | convolution fusion | flops 136708096 | bytes 5521409 | tf_op jit(solution)/shard_map/while/body/eval_jaxpr/hqk,khd->hqd/dot_general | solution.py:65
  136.8 3.4 %fusion.95 = (f32[4,512]{1,0:T(4,128)S(1)}, f32[4,512,512]{1,2,0:T(8,128)}) fusion(bf16[512,4,32]{0,2,1:T(8,128)(2,1)S(1)} %get-tuple-element.228, bf16[8,512,32]{1,2,0:T(8,128)(2,1)} %get-tuple-element.227, s32[]{:T(128)S(6)} %copy.43, f32[4,512,512]{2,1,0:T(8,128)S(1)} %fusion.94), kind=kOutput, calls=%fused_computation.113.clone.1 | convolution fusion | flops 70252544 | bytes 8560644 | tf_op jit(solution)/shard_map/while/body/eval_jaxpr/qhr,kr->hqk/dot_general | solution.py:59
  143.2 3.0 %fusion.98 = f32[4,512,64]{1,2,0:T(8,128)S(1)} fusion(bf16[512,4,64]{0,2,1:T(8,128)(2,1)S(1)} %bitcast.80, f32[4,512,512]{1,2,0:T(8,128)} %get-tuple-element.195, f32[4,512]{1,0:T(4,128)S(1)} %select_maximum_fusion.2, f32[4,512,64]{1,2,0:T(8,128)S(1)} %get-tuple-element.213, f32[4,512]{1,0:T(4,128)S(1)} %get-tuple-element.198, pred[]{:T(512)S(6)} %compare.7), kind=kOutput, calls=%fused_computation.10.clone.1 | convolution fusion | flops 136708096 | bytes 5521409 | tf_op jit(solution)/shard_map/while/body/eval_jaxpr/hqk,khd->hqd/dot_general | solution.py:65
  148.2 3.4 %fusion.95 = (f32[4,512]{1,0:T(4,128)S(1)}, f32[4,512,512]{1,2,0:T(8,128)}) fusion(bf16[512,4,32]{0,2,1:T(8,128)(2,1)S(1)} %get-tuple-element.228, bf16[8,512,32]{1,2,0:T(8,128)(2,1)} %get-tuple-element.227, s32[]{:T(128)S(6)} %copy.43, f32[4,512,512]{2,1,0:T(8,128)S(1)} %fusion.94), kind=kOutput, calls=%fused_computation.113.clone.1 | convolution fusion | flops 70252544 | bytes 8560644 | tf_op jit(solution)/shard_map/while/body/eval_jaxpr/qhr,kr->hqk/dot_general | solution.py:59
  154.6 3.0 %fusion.98 = f32[4,512,64]{1,2,0:T(8,128)S(1)} fusion(bf16[512,4,64]{0,2,1:T(8,128)(2,1)S(1)} %bitcast.80, f32[4,512,512]{1,2,0:T(8,128)} %get-tuple-element.195, f32[4,512]{1,0:T(4,128)S(1)} %select_maximum_fusion.2, f32[4,512,64]{1,2,0:T(8,128)S(1)} %get-tuple-element.213, f32[4,512]{1,0:T(4,128)S(1)} %get-tuple-element.198, pred[]{:T(512)S(6)} %compare.7), kind=kOutput, calls=%fused_computation.10.clone.1 | convolution fusion | flops 136708096 | bytes 5521409 | tf_op jit(solution)/shard_map/while/body/eval_jaxpr/hqk,khd->hqd/dot_general | solution.py:65
  159.7 3.4 %fusion.95 = (f32[4,512]{1,0:T(4,128)S(1)}, f32[4,512,512]{1,2,0:T(8,128)}) fusion(bf16[512,4,32]{0,2,1:T(8,128)(2,1)S(1)} %get-tuple-element.228, bf16[8,512,32]{1,2,0:T(8,128)(2,1)} %get-tuple-element.227, s32[]{:T(128)S(6)} %copy.43, f32[4,512,512]{2,1,0:T(8,128)S(1)} %fusion.94), kind=kOutput, calls=%fused_computation.113.clone.1 | convolution fusion | flops 70252544 | bytes 8560644 | tf_op jit(solution)/shard_map/while/body/eval_jaxpr/qhr,kr->hqk/dot_general | solution.py:59
  171.1 3.4 %fusion.95 = (f32[4,512]{1,0:T(4,128)S(1)}, f32[4,512,512]{1,2,0:T(8,128)}) fusion(bf16[512,4,32]{0,2,1:T(8,128)(2,1)S(1)} %get-tuple-element.228, bf16[8,512,32]{1,2,0:T(8,128)(2,1)} %get-tuple-element.227, s32[]{:T(128)S(6)} %copy.43, f32[4,512,512]{2,1,0:T(8,128)S(1)} %fusion.94), kind=kOutput, calls=%fused_computation.113.clone.1 | convolution fusion | flops 70252544 | bytes 8560644 | tf_op jit(solution)/shard_map/while/body/eval_jaxpr/qhr,kr->hqk/dot_general | solution.py:59
  177.5 3.0 %fusion.98 = f32[4,512,64]{1,2,0:T(8,128)S(1)} fusion(bf16[512,4,64]{0,2,1:T(8,128)(2,1)S(1)} %bitcast.80, f32[4,512,512]{1,2,0:T(8,128)} %get-tuple-element.195, f32[4,512]{1,0:T(4,128)S(1)} %select_maximum_fusion.2, f32[4,512,64]{1,2,0:T(8,128)S(1)} %get-tuple-element.213, f32[4,512]{1,0:T(4,128)S(1)} %get-tuple-element.198, pred[]{:T(512)S(6)} %compare.7), kind=kOutput, calls=%fused_computation.10.clone.1 | convolution fusion | flops 136708096 | bytes 5521409 | tf_op jit(solution)/shard_map/while/body/eval_jaxpr/hqk,khd->hqd/dot_general | solution.py:65
  182.5 3.4 %fusion.95 = (f32[4,512]{1,0:T(4,128)S(1)}, f32[4,512,512]{1,2,0:T(8,128)}) fusion(bf16[512,4,32]{0,2,1:T(8,128)(2,1)S(1)} %get-tuple-element.228, bf16[8,512,32]{1,2,0:T(8,128)(2,1)} %get-tuple-element.227, s32[]{:T(128)S(6)} %copy.43, f32[4,512,512]{2,1,0:T(8,128)S(1)} %fusion.94), kind=kOutput, calls=%fused_computation.113.clone.1 | convolution fusion | flops 70252544 | bytes 8560644 | tf_op jit(solution)/shard_map/while/body/eval_jaxpr/qhr,kr->hqk/dot_general | solution.py:59
  193.9 3.4 %fusion.95 = (f32[4,512]{1,0:T(4,128)S(1)}, f32[4,512,512]{1,2,0:T(8,128)}) fusion(bf16[512,4,32]{0,2,1:T(8,128)(2,1)S(1)} %get-tuple-element.228, bf16[8,512,32]{1,2,0:T(8,128)(2,1)} %get-tuple-element.227, s32[]{:T(128)S(6)} %copy.43, f32[4,512,512]{2,1,0:T(8,128)S(1)} %fusion.94), kind=kOutput, calls=%fused_computation.113.clone.1 | convolution fusion | flops 70252544 | bytes 8560644 | tf_op jit(solution)/shard_map/while/body/eval_jaxpr/qhr,kr->hqk/dot_general | solution.py:59
  205.6 4.3 %all-to-all-start.1 = ((bf16[8,48,512]{2,1,0:T(8,128)(2,1)}), bf16[8,48,512]{2,1,0:T(8,128)(2,1)S(1)}, u32[]{:S(2)}, u32[]{:S(2)}) async-start(bf16[8,48,512]{2,1,0:T(8,128)(2,1)} %bitcast.92), calls=%async_computation.3 | async-start | bytes 786432 | tf_op jit(solution)/shard_map/all_to_all | solution.py:177
  210.3 12.2 %all-to-all-done.1 = bf16[8,48,512]{2,1,0:T(8,128)(2,1)S(1)} async-done(((bf16[8,48,512]{2,1,0:T(8,128)(2,1)}), bf16[8,48,512]{2,1,0:T(8,128)(2,1)S(1)}, u32[]{:S(2)}, u32[]{:S(2)}) %all-to-all-start.1) | async-done | bytes 393248 | tf_op jit(solution)/shard_map/all_to_all | solution.py:177
  225.3 15.2 %reduce-scatter.3.cloned.1.call-done = bf16[128,2048]{1,0:T(8,128)(2,1)} async-done(((bf16[512,2048]{1,0:T(8,128)(2,1)}), bf16[128,2048]{1,0:T(8,128)(2,1)}) %reduce-scatter.3.cloned.1.call-update) | async-done | bytes 524304 | tf_op jit(solution)/shard_map/reduce_scatter | solution.py:136
  (175 shorter events, 82.7 us)
Async XLA Ops:
  8.0 195.4 %copy-start = (bf16[256,2048]{1,0:T(8,128)(2,1)S(1)}, bf16[256,2048]{1,0:T(8,128)(2,1)}, u32[]{:S(2)}) copy-start(bf16[256,2048]{1,0:T(8,128)(2,1)} %param.28) | copy-start | bytes 3145732
  8.0 95.7 %all-gather.2.cloned.1.call-start = ((), (), s32[]{:S(2)}) async-start(), calls=%async_computation.4 | async-start | bytes 2359296 | tf_op jit(solution)/shard_map/all_gather | solution.py:126
  13.5 11.9 %copy-start.9 = (bf16[512]{0:T(512)(128)(2,1)S(1)}, bf16[512]{0:T(512)(128)(2,1)}, u32[]{:S(2)}) copy-start(bf16[512]{0:T(512)(128)(2,1)} %param.22) | copy-start | bytes 3076
  13.5 11.9 %copy-start.2 = (bf16[512,512]{1,0:T(8,128)(2,1)S(1)}, bf16[512,512]{1,0:T(8,128)(2,1)}, u32[]{:S(2)}) copy-start(bf16[512,512]{1,0:T(8,128)(2,1)} %param.19) | copy-start | bytes 1572868
  15.1 10.5 %copy-start.5 = (bf16[512,32]{0,1:T(8,128)(2,1)S(1)}, bf16[512,32]{0,1:T(8,128)(2,1)}, u32[]{:S(2)}) copy-start(bf16[512,32]{0,1:T(8,128)(2,1)} %param.21) | copy-start | bytes 98308
  16.4 41.6 %copy-start.11 = (bf16[512,128]{1,0:T(8,128)(2,1)S(1)}, bf16[512,128]{1,0:T(8,128)(2,1)}, u32[]{:S(2)}) copy-start(bf16[512,128]{1,0:T(8,128)(2,1)} %param.25) | copy-start | bytes 393220
  19.0 37.5 %all-to-all-start = ((bf16[8,48,512]{2,1,0:T(8,128)(2,1)}), bf16[8,48,512]{2,1,0:T(8,128)(2,1)S(1)}, u32[]{:S(2)}, u32[]{:S(2)}) async-start(bf16[8,48,512]{2,1,0:T(8,128)(2,1)} %bitcast.12), calls=%async_computation.1 | async-start | bytes 786432 | tf_op jit(solution)/shard_map/all_to_all | solution.py:163
  25.3 180.3 %reduce-scatter.5.cloned.1.call-start = ((), (), s32[]{:S(2)}) async-start(), calls=%async_computation.6 | async-start | bytes 1966080 | tf_op jit(solution)/shard_map/reduce_scatter | solution.py:173
  25.4 33.7 %copy-start.7 = (f32[512]{0:T(512)}, f32[512]{0:T(512)S(1)}, u32[]{:S(2)}) copy-start(f32[512]{0:T(512)S(1)} %convert_element_type.96) | copy-start | bytes 6148
  25.6 33.5 %copy-start.8 = (f32[512]{0:T(512)}, f32[512]{0:T(512)S(1)}, u32[]{:S(2)}) copy-start(f32[512]{0:T(512)S(1)} %add_rsqrt_fusion.1) | copy-start | bytes 6148
  56.5 12.3 %collective-permute-start = (bf16[384,512]{1,0:T(8,128)(2,1)S(1)}, bf16[384,512]{1,0:T(8,128)(2,1)S(1)}, u32[]{:S(2)}, u32[]{:S(2)}) collective-permute-start(bf16[384,512]{1,0:T(8,128)(2,1)S(1)} %bitcast.84), channel_id=1, source_target_pairs={{0,1},{1,2},{2,3},{3,0},{4,5},{5,6},{6,7},{7,4},{8,9},{9,10},{10,1... | collective-permute-start | bytes 1179656 | tf_op jit(solution)/shard_map/ppermute | solution.py:17
  68.8 11.4 %collective-permute-start.1 = (bf16[384,512]{1,0:T(8,128)(2,1)S(1)}, bf16[384,512]{1,0:T(8,128)(2,1)S(1)}, u32[]{:S(2)}, u32[]{:S(2)}) collective-permute-start(bf16[384,512]{1,0:T(8,128)(2,1)S(1)} %collective-permute-done), channel_id=1, source_target_pairs={{0,1},{1,2},{2,3},{3,0},{4,5},{5,6},{6,7},{7,4},{8,9},{9,10},{10,1... | collective-permute-start | bytes 1179656 | tf_op jit(solution)/shard_map/ppermute | solution.py:17
  80.2 10.6 %collective-permute-start.2 = (bf16[384,512]{1,0:T(8,128)(2,1)S(1)}, bf16[384,512]{1,0:T(8,128)(2,1)S(1)}, u32[]{:S(2)}, u32[]{:S(2)}) collective-permute-start(bf16[384,512]{1,0:T(8,128)(2,1)S(1)} %collective-permute-done.1), channel_id=1, source_target_pairs={{0,1},{1,2},{2,3},{3,0},{4,5},{5,6},{6,7},{7,4},{8,9},{9,10},{10,1... | collective-permute-start | bytes 1179656 | tf_op jit(solution)/shard_map/ppermute | solution.py:17
  84.9 7.9 %copy-start.10 = (bf16[1,2048,1024]{2,1,0:T(8,128)(2,1)S(1)}, bf16[1,2048,1024]{2,1,0:T(8,128)(2,1)}, u32[]{:S(2)}) copy-start(bf16[1,2048,1024]{2,1,0:T(8,128)(2,1)} %param.33) | copy-start | bytes 12582916
  91.2 1.7 copy-start.4
  103.5 2.7 %copy-start.12 = (bf16[256,256]{1,0:T(8,128)(2,1)S(1)}, bf16[256,256]{1,0:T(8,128)(2,1)}, u32[]{:S(2)}) copy-start(bf16[256,256]{1,0:T(8,128)(2,1)} %param.26) | copy-start | bytes 393220
  103.5 2.7 %copy-start.14 = (f32[256]{0:T(256)S(1)}, f32[256]{0:T(256)}, u32[]{:S(2)}) copy-start(f32[256]{0:T(256)} %convert_element_type.92) | copy-start | bytes 3076
  103.5 6.4 %copy-start.13 = (bf16[256,256]{1,0:T(8,128)(2,1)S(1)}, bf16[256,256]{1,0:T(8,128)(2,1)}, u32[]{:S(2)}) copy-start(bf16[256,256]{1,0:T(8,128)(2,1)} %param.27) | copy-start | bytes 393220
  103.5 137.0 %reduce-scatter.3.cloned.1.call-start = ((), (), s32[]{:S(2)}) async-start(), calls=%async_computation.5 | async-start | bytes 2621440 | tf_op jit(solution)/shard_map/reduce_scatter | solution.py:136
  103.8 6.1 %copy-start.1 = (bf16[4096,256]{1,0:T(8,128)(2,1)S(1)}, bf16[4096,256]{1,0:T(8,128)(2,1)}, u32[]{:S(2)}) copy-start(bf16[4096,256]{1,0:T(8,128)(2,1)} %all-gather.2.cloned.1.call-done) | copy-start | bytes 6291460
  203.4 6.5 %copy-start.3 = (s32[128,2]{1,0:T(8,128)S(1)}, s32[128,2]{1,0:T(8,128)}, u32[]{:S(2)}) copy-start(s32[128,2]{1,0:T(8,128)} %get-tuple-element.128) | copy-start | bytes 3076
  203.4 6.6 %copy-start.6 = (f32[128,2]{0,1:T(2,128)S(1)}, f32[128,2]{0,1:T(2,128)}, u32[]{:S(2)}) copy-start(f32[128,2]{0,1:T(2,128)} %param.32) | copy-start | bytes 3076
  205.6 16.8 %all-to-all-start.1 = ((bf16[8,48,512]{2,1,0:T(8,128)(2,1)}), bf16[8,48,512]{2,1,0:T(8,128)(2,1)S(1)}, u32[]{:S(2)}, u32[]{:S(2)}) async-start(bf16[8,48,512]{2,1,0:T(8,128)(2,1)} %bitcast.92), calls=%async_computation.3 | async-start | bytes 786432 | tf_op jit(solution)/shard_map/all_to_all | solution.py:177
Sparse Core Ops, SparseCore 0:
  10.4 42.0 all-gather.1
Sparse Core Ops, SparseCore 1:
  103.6 30.7 reduce-scatter.4
  205.7 34.8 reduce-scatter.2
